TPU v7x, 32 devices: a whole 2x2x4 slice. The times are simulated.
32 devices in a mesh: sp: 8 (over z, y), tp: 4 (over x, core).
Axes of the slice: x: 2, y: 2, z: 4, core: 2. Of those that a mesh axis runs over, the one named last changes fastest.
Arguments:
- tokens: bfloat16 [2048, 2048], P(('sp', 'tp')), may hold values from -6 to 6
- norm_gain: float32 [2048], replicated, may hold values from 0.1 to 1.9
- ret_query: bfloat16 [2048, 1024], P('sp', 'tp'), may hold values from -0.125 to 0.125
- ret_key: bfloat16 [2048, 1024], P('sp', 'tp'), may hold values from -0.125 to 0.125
- ret_value: bfloat16 [2048, 2048], P('sp', 'tp'), may hold values from -0.125 to 0.125
- log_decay: float32 [8, 2048], P('tp', 'sp'), may hold values from -2 to 0, as said below
- att_query: bfloat16 [2048, 2048], P('sp', 'tp')
- att_key: bfloat16 [2048, 256], P('sp', 'tp')
- att_value: bfloat16 [2048, 256], P('sp', 'tp'), may hold values from -0.125 to 0.125
- sink_logits: float32 [32], P('tp'), may hold values from 3 to 6
- ret_out: bfloat16 [2048, 2048], P('tp', 'sp'), may hold values from -0.125 to 0.125
- att_out: bfloat16 [2048, 2048], P('tp', 'sp'), may hold values from -1 to 1
Outputs:
- mixed: bfloat16 [2048, 2048], P(('sp', 'tp'))
Inputs may be any that keep to these rules, and one draw needn't show every extreme that they name: `log_decay`: strictly negative.
All inputs are finite; a program needn't handle non-finite values.
Results may differ from a plain program's by a relative error of at most 0.013.
Values may be sent and summed in bfloat16 or wider, within the bound.
A program may use at most 128 MiB of HBM per device.

v0:
```python
import jax
import jax.numpy as jnp
from jax import lax
from jax.sharding import PartitionSpec as P

RETAIN_KEY_SIZE = 128
V_DIM = 256
HEAD_DIM = 64
WINDOW = 128
BLOCK = 128


epsilon = 1e-05
rope_base = 10000.0
masked_out = -1e30


def prefix(part, axis, combine, identity):
    place = lax.axis_index(axis)
    gathered = jax.tree.map(lambda a: lax.all_gather(a, axis), part)
    state = jax.tree.map(lambda a, e: jnp.zeros_like(a) + jnp.asarray(e, a.dtype), part, identity)

    def one(lap, state):
        return combine(
            state, jax.tree.map(lambda a: lax.dynamic_index_in_dim(a, lap, 0, False), gathered)
        )

    return lax.fori_loop(0, place, one, state)


def shifted(value, axis, steps):
    count = lax.axis_size(axis)
    initial, last = (max(0, -steps), min(count, count - steps))
    return lax.ppermute(value, axis, [(source, source + steps) for source in range(initial, last)])


def rotate(values, positions):
    half_dim = values.shape[-1] // 2
    inverse = rope_base ** (-jnp.arange(half_dim, dtype=jnp.float32) / half_dim)
    angles = positions.astype(jnp.float32)[:, None] * inverse[None, :]
    cosine = jnp.cos(angles)[:, None, :]
    sine_part = jnp.sin(angles)[:, None, :]
    first_half = values[..., :half_dim].astype(jnp.float32)
    second_half = values[..., half_dim:].astype(jnp.float32)
    return jnp.concatenate(
        [
            first_half * cosine - second_half * sine_part,
            second_half * cosine + first_half * sine_part,
        ],
        axis=-1,
    )


def chain_join(earlier_part, later_part):
    return (
        earlier_part[0] * later_part[0],
        later_part[0][:, None, None] * earlier_part[1] + later_part[1],
    )


def retention_path(query_ret, key_ret, value_ret, log_decay):
    tok_count, heads_here = (query_ret.shape[0], query_ret.shape[1])
    blocks = tok_count // BLOCK
    q_blocks = query_ret.reshape(blocks, BLOCK, heads_here, RETAIN_KEY_SIZE)
    k_blocks = key_ret.reshape(blocks, BLOCK, heads_here, RETAIN_KEY_SIZE)
    v_blocks = value_ret.reshape(blocks, BLOCK, heads_here, V_DIM)
    running = jnp.cumsum(log_decay.reshape(heads_here, blocks, BLOCK), axis=-1)
    closing = running[:, :, -1:]
    within = running[:, :, :, None] - running[:, :, None, :]
    causal_mask = jnp.arange(BLOCK)[:, None] >= jnp.arange(BLOCK)[None, :]
    weighting = jnp.where(causal_mask, jnp.exp(jnp.minimum(within, 0.0)), 0.0)
    scores = (
        jnp.einsum("nihd,njhd->hnij", q_blocks, k_blocks, preferred_element_type=jnp.float32)
        * weighting
    )
    in_block = jnp.einsum(
        "hnij,njhv->nihv", scores.astype(jnp.bfloat16), v_blocks, preferred_element_type=jnp.float32
    )
    key_fade = (
        k_blocks.astype(jnp.float32) * jnp.exp(closing - running).transpose(1, 2, 0)[..., None]
    ).astype(jnp.bfloat16)
    contrib = jnp.einsum("njhd,njhv->nhdv", key_fade, v_blocks, preferred_element_type=jnp.float32)
    block_fade = jnp.exp(closing[:, :, 0]).T

    def advance(carried, entry_pair):
        addend, factor = entry_pair
        return (carried * factor[:, None, None] + addend, carried)

    final_state, before = lax.scan(
        advance, jnp.zeros((heads_here, RETAIN_KEY_SIZE, V_DIM), jnp.float32), (contrib, block_fade)
    )
    device_fade = jnp.exp(jnp.sum(closing[:, :, 0], axis=1))
    identity = (jnp.ones_like(device_fade), jnp.zeros_like(final_state))
    arrived = prefix((device_fade, final_state), "sp", chain_join, identity)
    leading = jnp.cumsum(closing[:, :, 0], axis=1) - closing[:, :, 0]
    before = before + arrived[1][None] * jnp.exp(leading).T[:, :, None, None]
    query_fade = (
        q_blocks.astype(jnp.float32) * jnp.exp(running).transpose(1, 2, 0)[..., None]
    ).astype(jnp.bfloat16)
    carried_term = jnp.einsum(
        "nihd,nhdv->nihv", query_fade.astype(jnp.float32), before, precision=lax.Precision.HIGHEST
    )
    final_product = in_block + carried_term
    final_product = final_product * lax.rsqrt(
        jnp.mean(final_product * final_product, axis=-1, keepdims=True) + epsilon
    )
    return final_product.reshape(tok_count, heads_here * V_DIM).astype(jnp.bfloat16)


def attention_path(query_att, key_att, value_att, sink_logits, anchor):
    tok_count = query_att.shape[0]
    kv_here = key_att.shape[1] // HEAD_DIM
    group_size = query_att.shape[1] // (kv_here * HEAD_DIM)
    stacked = jnp.concatenate([key_att, value_att], axis=1)
    window_rim = shifted(stacked[tok_count - WINDOW :], "sp", 1)
    blocks = tok_count // WINDOW
    extended = jnp.concatenate([window_rim, stacked], axis=0).reshape(
        blocks + 1, WINDOW, 2, kv_here, HEAD_DIM
    )
    paired = jnp.concatenate([extended[:-1], extended[1:]], axis=1)
    keys_pair = paired[:, :, 0]
    values_pair = paired[:, :, 1]
    q_blocks = query_att.reshape(blocks, WINDOW, kv_here, group_size, HEAD_DIM)
    scores = jnp.einsum(
        "nihgd,njhd->nhgij", q_blocks, keys_pair, preferred_element_type=jnp.float32
    ) * HEAD_DIM ** (-0.5)
    query_pos = anchor + (jnp.arange(blocks) * WINDOW)[:, None] + jnp.arange(WINDOW)[None, :]
    key_pos = (
        anchor + (jnp.arange(blocks) * WINDOW - WINDOW)[:, None] + jnp.arange(2 * WINDOW)[None, :]
    )
    allowed = (
        (key_pos[:, None, :] >= 0)
        & (key_pos[:, None, :] <= query_pos[:, :, None])
        & (query_pos[:, :, None] - key_pos[:, None, :] < WINDOW)
    )
    scores = jnp.where(allowed[:, None, None], scores, masked_out)
    sink_logit = sink_logits.reshape(kv_here, group_size)[None, :, :, None]
    highest = jnp.maximum(jnp.max(scores, axis=-1), sink_logit)
    lifted = jnp.exp(scores - highest[..., None])
    denominator = jnp.sum(lifted, axis=-1) + jnp.exp(sink_logit - highest)
    attn_weights = (lifted / denominator[..., None]).astype(jnp.bfloat16)
    final_product = jnp.einsum(
        "nhgij,njhd->nihgd", attn_weights, values_pair, preferred_element_type=jnp.float32
    )
    return final_product.reshape(tok_count, kv_here * group_size * HEAD_DIM).astype(jnp.bfloat16)


def on_device(
    tokens,
    norm_gain,
    ret_query,
    ret_key,
    ret_value,
    log_decay,
    att_query,
    att_key,
    att_value,
    sink_logits,
    ret_out,
    att_out,
):
    tok_float = tokens.astype(jnp.float32)
    normed = (
        tok_float
        * lax.rsqrt(jnp.mean(tok_float * tok_float, axis=-1, keepdims=True) + epsilon)
        * norm_gain
    ).astype(jnp.bfloat16)
    weights = (ret_query, ret_key, ret_value, att_query, att_key, att_value)
    widths = [weight.shape[1] for weight in weights]
    points = [sum(widths[:index]) for index in range(1, len(widths))]
    gathered = (
        lax.all_gather(weights[0], "sp", axis=0, tiled=True),
        lax.all_gather(weights[1], "sp", axis=0, tiled=True),
        lax.all_gather(weights[2], "sp", axis=0, tiled=True),
        lax.all_gather(weights[3], "sp", axis=0, tiled=True),
        lax.all_gather(weights[4], "sp", axis=0, tiled=True),
        lax.all_gather(weights[5], "sp", axis=0, tiled=True),
    )
    joined = jnp.concatenate(gathered, axis=1)
    projected = jnp.dot(
        lax.all_gather(normed, "tp", axis=0, tiled=True), joined, preferred_element_type=jnp.float32
    ).astype(jnp.bfloat16)
    sections = jnp.split(projected, points, axis=1)
    tok_count = sections[0].shape[0]
    anchor = lax.axis_index("sp") * tok_count
    positions = anchor + jnp.arange(tok_count, dtype=jnp.int32)
    query_ret = rotate(sections[0].reshape(tok_count, -1, RETAIN_KEY_SIZE), positions).astype(
        jnp.bfloat16
    )
    key_ret = (
        rotate(sections[1].reshape(tok_count, -1, RETAIN_KEY_SIZE), positions)
        * RETAIN_KEY_SIZE ** (-0.5)
    ).astype(jnp.bfloat16)
    value_ret = sections[2].reshape(tok_count, -1, V_DIM)
    ret_mix = retention_path(query_ret, key_ret, value_ret, log_decay)
    att_mix = attention_path(sections[3], sections[4], sections[5], sink_logits, anchor)
    out_whole = (
        lax.all_gather(ret_out, "sp", axis=1, tiled=True),
        lax.all_gather(att_out, "sp", axis=1, tiled=True),
    )
    return lax.psum_scatter(
        (
            jnp.dot(ret_mix, out_whole[0], preferred_element_type=jnp.float32)
            + jnp.dot(att_mix, out_whole[1], preferred_element_type=jnp.float32)
        ).astype(jnp.bfloat16),
        "tp",
        scatter_dimension=0,
        tiled=True,
    )


def solution(mesh):
    in_specs = (
        P(("sp", "tp"), None),
        P(),
        P("sp", "tp"),
        P("sp", "tp"),
        P("sp", "tp"),
        P("tp", "sp"),
        P("sp", "tp"),
        P("sp", "tp"),
        P("sp", "tp"),
        P("tp"),
        P("tp", "sp"),
        P("tp", "sp"),
    )
    out_specs = P(("sp", "tp"), None)
    return jax.shard_map(
        on_device, mesh=mesh, in_specs=in_specs, out_specs=out_specs, check_vma=False
    )
```

profile of v0, /device:TPU:0, one launch (start us, length us, event | category | flops | bytes accessed | tf_op | source)
XLA Modules:
  0.0 403.3 jit_solution(18088463393501126298)
XLA Ops:
  6.5 0.7 all-gather.13.cloned.1.call-update
  7.3 0.7 all-gather.15.cloned.1.call-update
  8.1 0.7 all-gather.17.cloned.1.call-update
  8.8 0.5 all-gather.19.cloned.1.call-update
  9.4 1.1 fusion.7
  10.5 1.8 fusion.9
  12.4 33.4 %all_gather.42 = bf16[2048,64]{0,1:T(8,128)(2,1)S(1)} all-gather(bf16[256,64]{0,1:T(8,128)(2,1)} %param.23), channel_id=1, replica_groups=mesh['sp'=8,'tp'=4] {'sp'}, dimensions={0}, use_global_device_ids=true | all-gather | bytes 294912 | tf_op jit(solution)/shard_map/all_gather | solution.py:176
  46.1 31.0 %all_gather.43 = bf16[2048,64]{0,1:T(8,128)(2,1)S(1)} all-gather(bf16[256,64]{0,1:T(8,128)(2,1)S(1)} %copy-done.1), channel_id=1, replica_groups=mesh['sp'=8,'tp'=4] {'sp'}, dimensions={0}, use_global_device_ids=true | all-gather | bytes 294912 | tf_op jit(solution)/shard_map/all_gather | solution.py:177
  77.4 0.6 reduce_window_sum.24
  78.9 16.2 %all-gather.15.cloned.1.call-done = bf16[2048,256]{1,0:T(8,128)(2,1)} async-done(((bf16[256,256]{1,0:T(8,128)(2,1)}), bf16[2048,256]{1,0:T(8,128)(2,1)}) %all-gather.15.cloned.1.call-update) | async-done | bytes 1048592 | tf_op jit(solution)/shard_map/all_gather | solution.py:173
  95.1 50.0 %all-gather.17.cloned.1.call-done = bf16[2048,512]{1,0:T(8,128)(2,1)} async-done(((bf16[256,512]{1,0:T(8,128)(2,1)}), bf16[2048,512]{1,0:T(8,128)(2,1)}) %all-gather.17.cloned.1.call-update) | async-done | bytes 2097168 | tf_op jit(solution)/shard_map/all_gather | solution.py:174
  145.1 49.6 %all-gather.19.cloned.1.call-done = bf16[2048,512]{1,0:T(8,128)(2,1)} async-done(((bf16[256,512]{1,0:T(8,128)(2,1)}), bf16[2048,512]{1,0:T(8,128)(2,1)}) %all-gather.19.cloned.1.call-update) | async-done | bytes 2097168 | tf_op jit(solution)/shard_map/all_gather | solution.py:175
  194.7 11.2 %concatenate.29 = bf16[2048,1664]{1,0:T(8,128)(2,1)} concatenate(bf16[2048,256]{1,0:T(8,128)(2,1)} %all-gather.13.cloned.1.call-done, bf16[2048,256]{1,0:T(8,128)(2,1)} %all-gather.15.cloned.1.call-done, bf16[2048,512]{1,0:T(8,128)(2,1)} %all-gather.17.cloned.1.call-done, bf16[2048,512]{1,0:T(8,128)(2,1)} %all-gather.19.cloned.1.call-done, bf16[2048,64]{1,0:T(8,128)(2,1)S(1)} %copy.52, ...), dimensions={1} | concatenate | bytes 13631488 | tf_op jit(solution)/shard_map/concatenate | solution.py:179
  206.0 5.4 %all-gather.11.cloned.1.call-done = bf16[256,2048]{1,0:T(8,128)(2,1)} async-done(((bf16[64,2048]{1,0:T(8,128)(2,1)}), bf16[256,2048]{1,0:T(8,128)(2,1)}) %all-gather.11.cloned.1.call-update) | async-done | bytes 1048592 | tf_op jit(solution)/shard_map/all_gather | solution.py:181
  211.4 5.3 %convolution_convert_fusion = bf16[256,1664]{1,0:T(8,128)(2,1)S(1)} fusion(bf16[256,2048]{1,0:T(8,128)(2,1)} %all-gather.11.cloned.1.call-done, bf16[2048,1664]{1,0:T(8,128)(2,1)} %concatenate.29), kind=kOutput, calls=%fused_computation.8 | convolution fusion | flops 1745256448 | bytes 8716288 | tf_op jit(solution)/shard_map/dot_general | solution.py:180
  217.8 0.4 fusion.25
  218.5 0.7 copy-done
  219.3 0.7 all-gather.21.cloned.1.call-update
  220.0 0.7 all-gather.23.cloned.1.call-update
  221.0 0.6 dynamic-slice
  222.6 3.4 collective-permute-start
  226.0 19.7 %all-reduce = f32[16]{0:T(128)S(1)} all-reduce(f32[16]{0:T(128)S(1)} %exponential_dynamic-update-slice_fusion), channel_id=2, replica_groups=mesh['sp'=8,'tp'=4] {'sp'}, use_global_device_ids=true, to_apply=%add | all-reduce | flops 16 | bytes 128
  246.9 0.5 fusion.55
  247.9 0.5 fusion.4
  248.7 20.1 %all-gather.25.cloned.1.call-done = f32[16,128,256]{2,1,0:T(8,128)} async-done(((f32[2,128,256]{2,1,0:T(8,128)}), f32[16,128,256]{2,1,0:T(8,128)}) %all-gather.25.cloned.1.call-update) | async-done | bytes 2097168 | tf_op jit(solution)/shard_map/all_gather | solution.py:20
  268.8 0.8 fusion.11
  269.6 0.5 multiply_reduce_fusion
  270.4 49.4 %all-gather.21.cloned.1.call-done = bf16[512,2048]{1,0:T(8,128)(2,1)} async-done(((bf16[512,256]{1,0:T(8,128)(2,1)}), bf16[512,2048]{1,0:T(8,128)(2,1)}) %all-gather.21.cloned.1.call-update) | async-done | bytes 2097168 | tf_op jit(solution)/shard_map/all_gather | solution.py:198
  319.7 2.3 fusion.56
  322.0 48.3 %all-gather.23.cloned.1.call-done = bf16[512,2048]{1,0:T(8,128)(2,1)} async-done(((bf16[512,256]{1,0:T(8,128)(2,1)}), bf16[512,2048]{1,0:T(8,128)(2,1)}) %all-gather.23.cloned.1.call-update) | async-done | bytes 2097168 | tf_op jit(solution)/shard_map/all_gather | solution.py:199
  370.3 3.3 fusion.1
  373.7 23.1 %reduce-scatter.2.cloned.1.call-done = bf16[64,2048]{1,0:T(8,128)(2,1)} async-done(((bf16[256,2048]{1,0:T(8,128)(2,1)}), bf16[64,2048]{1,0:T(8,128)(2,1)}) %reduce-scatter.2.cloned.1.call-update) | async-done | bytes 262160 | tf_op jit(solution)/shard_map/reduce_scatter | solution.py:201
  (90 shorter events, 6.1 us)
Async XLA Ops:
  6.5 39.5 %copy-start.1 = (bf16[256,64]{0,1:T(8,128)(2,1)S(1)}, bf16[256,64]{0,1:T(8,128)(2,1)}, u32[]{:S(2)}) copy-start(bf16[256,64]{0,1:T(8,128)(2,1)} %param.24) | copy-start | bytes 98308
  6.5 70.8 %copy-start.3 = (f32[2,256]{1,0:T(2,128)S(1)}, f32[2,256]{1,0:T(2,128)}, u32[]{:S(2)}) copy-start(f32[2,256]{1,0:T(2,128)} %param.21) | copy-start | bytes 6148
  6.5 72.4 %all-gather.13.cloned.1.call-start = ((), (), s32[]{:S(2)}) async-start(), calls=%async_computation.2 | async-start | bytes 1179648 | tf_op jit(solution)/shard_map/all_gather | solution.py:172
  7.3 87.9 %all-gather.15.cloned.1.call-start = ((), (), s32[]{:S(2)}) async-start(), calls=%async_computation.3 | async-start | bytes 1179648 | tf_op jit(solution)/shard_map/all_gather | solution.py:173
  8.0 137.1 %all-gather.17.cloned.1.call-start = ((), (), s32[]{:S(2)}) async-start(), calls=%async_computation.4 | async-start | bytes 2359296 | tf_op jit(solution)/shard_map/all_gather | solution.py:174
  8.7 186.0 %all-gather.19.cloned.1.call-start = ((), (), s32[]{:S(2)}) async-start(), calls=%async_computation.5 | async-start | bytes 2359296 | tf_op jit(solution)/shard_map/all_gather | solution.py:175
  9.3 202.1 %all-gather.11.cloned.1.call-start = ((), (), s32[]{:S(2)}) async-start(), calls=%async_computation.1 | async-start | bytes 1310720 | tf_op jit(solution)/shard_map/all_gather | solution.py:181
  12.3 256.5 %all-gather.25.cloned.1.call-start = ((), (), s32[]{:S(2)}) async-start(), calls=%async_computation.9 | async-start | bytes 2359296 | tf_op jit(solution)/shard_map/all_gather | solution.py:20
  218.1 2.9 copy-start.4
  218.5 0.7 copy-start
  219.2 100.5 %all-gather.21.cloned.1.call-start = ((), (), s32[]{:S(2)}) async-start(), calls=%async_computation.6 | async-start | bytes 2359296 | tf_op jit(solution)/shard_map/all_gather | solution.py:198
  220.0 150.4 %all-gather.23.cloned.1.call-start = ((), (), s32[]{:S(2)}) async-start(), calls=%async_computation.7 | async-start | bytes 2359296 | tf_op jit(solution)/shard_map/all_gather | solution.py:199
  220.7 176.1 %reduce-scatter.2.cloned.1.call-start = ((), (), s32[]{:S(2)}) async-start(), calls=%async_computation.8 | async-start | bytes 1310720 | tf_op jit(solution)/shard_map/reduce_scatter | solution.py:201
  222.6 24.1 %collective-permute-start = (bf16[128,128]{1,0:T(8,128)(2,1)S(1)}, bf16[128,128]{1,0:T(8,128)(2,1)S(1)}, u32[]{:S(2)}, u32[]{:S(2)}) collective-permute-start(bf16[128,128]{1,0:T(8,128)(2,1)S(1)} %slice.52), channel_id=1, source_target_pairs={{0,4},{4,8},{8,12},{12,16},{16,20},{20,24},{24,28},{1,5},{5,9},{9,... | collective-permute-start | bytes 98312 | tf_op jit(solution)/shard_map/ppermute | solution.py:34
  246.3 1.1 copy-start.2
Sparse Core Ops, SparseCore 0:
  9.5 44.1 all-gather.12
  55.8 39.2 all-gather.14
  97.3 47.7 all-gather.16
  147.1 47.6 all-gather.18
  196.1 15.2 all-gather.10
  219.3 49.4 all-gather.24
  270.8 48.8 all-gather.20
  321.8 48.5 all-gather.22
  373.8 22.9 reduce-scatter.1
where the time goes:
time: 404 us; the launch traced here: 403 us
  waiting for transfers between devices  266 us (66%)
  blocking collectives  84.1 us (21%)
  local copies, waits for them, and re-layouts  15.8 us (4%)
  between operations  14.2 us (4%)
  matrix products  13.5 us (3%)
  other arithmetic  5.7 us (1%)
    all_gather x1, waiting for transfers between devices, on_device(): lax.all_gather(weights[2], 'sp', axis=0, tiled=True)  50 us
    all_gather x1, waiting for transfers between devices, on_device(): lax.all_gather(weights[3], 'sp', axis=0, tiled=True)  49.6 us
    all_gather x1, waiting for transfers between devices, on_device(): lax.all_gather(ret_out, 'sp', axis=1, tiled=True)  49.4 us
    all_gather x1, waiting for transfers between devices, on_device(): lax.all_gather(att_out, 'sp', axis=1, tiled=True)  48.3 us
    all_gather x1, blocking collectives, on_device(): lax.all_gather(weights[4], 'sp', axis=0, tiled=True)  33.4 us
    all_gather x1, blocking collectives, on_device(): lax.all_gather(weights[5], 'sp', axis=0, tiled=True)  31 us
    reduce_scatter x1, waiting for transfers between devices, on_device(): lax.psum_scatter((jnp.dot(ret_mix, out_whole[0], preferred_element_type=j...  23.1 us
    all_gather x1, waiting for transfers between devices, prefix(): gathered = jax.tree.map(lambda a: lax.all_gather(a, axis), part)  20.1 us
  transfers between devices with their start and end apart: 10, of which 8 were waited for; matrix products, arithmetic and copies ran while one was open for 6% of the time, Pallas kernels for 0%

commit v1 on v0

--- a/solution.py
+++ b/solution.py
@@ -1,7 +1,14 @@
+import functools
+
 import jax
 import jax.numpy as jnp
 from jax import lax
+from jax.experimental import pallas as pl
+from jax.experimental.pallas import tpu as pltpu
 from jax.sharding import PartitionSpec as P
+
+MESH = pl.DeviceIdType.MESH
+LANES = 128
 
 RETAIN_KEY_SIZE = 128
 V_DIM = 256
@@ -143,6 +150,245 @@
         "nhgij,njhd->nihgd", attn_weights, values_pair, preferred_element_type=jnp.float32
     )
     return final_product.reshape(tok_count, kv_here * group_size * HEAD_DIM).astype(jnp.bfloat16)
+
+
+def ring_spot(index, count):
+    half = count // 2
+    return jnp.where(lax.rem(index, 2) == 0, index // 2, count - 1 - index // 2)
+
+
+def ring_member(spot, count):
+    half = count // 2
+    return jnp.where(spot < half, 2 * spot, 2 * (count - 1 - spot) + 1)
+
+
+def project_kernel(n, n_tp, normed_ref, pack_ref, out_ref, rows_ref, held, total, sems, tok_sems):
+    sp, tp = lax.axis_index("sp"), lax.axis_index("tp")
+    depth, width = pack_ref.shape
+    count = normed_ref.shape[0]
+    half = n // 2
+    spot = ring_spot(sp, n)
+    ahead = ring_member(lax.rem(spot + 1, n), n)
+    behind = ring_member(lax.rem(spot + n - 1, n), n)
+
+    barrier = pltpu.get_barrier_semaphore()
+    for peer in (ahead, behind):
+        pl.semaphore_signal(barrier, inc=1, device_id=(peer, tp), device_id_type=MESH)
+    for step in range(1, n_tp):
+        pl.semaphore_signal(
+            barrier, inc=1, device_id=(sp, lax.rem(tp + step, n_tp)), device_id_type=MESH
+        )
+    pl.semaphore_wait(barrier, 2 + n_tp - 1)
+
+    def rows_of(member):
+        return pl.ds(pl.multiple_of(member * depth, depth), depth)
+
+    middle = (width // LANES + 1) // 2 * LANES
+    spans = (pl.ds(0, middle), pl.ds(middle, width - middle))
+
+    def owner(direction, distance):
+        shift = n - distance if direction == 0 else distance
+        return ring_member(lax.rem(spot + shift, n), n)
+
+    def send(direction, step, part):
+        member = owner(direction, step - 1)
+        source = pack_ref.at[:, spans[part]] if step == 1 else held.at[rows_of(member), spans[part]]
+        return pltpu.make_async_remote_copy(
+            src_ref=source,
+            dst_ref=held.at[rows_of(member), spans[part]],
+            send_sem=sems.at[0, direction, step - 1, part],
+            recv_sem=sems.at[1, direction, step - 1, part],
+            device_id=(ahead if direction == 0 else behind, tp),
+            device_id_type=MESH,
+        )
+
+    def arrival(direction, step, part):
+        member = owner(direction, step)
+        return pltpu.make_async_remote_copy(
+            src_ref=held.at[rows_of(member), spans[part]],
+            dst_ref=held.at[rows_of(member), spans[part]],
+            send_sem=sems.at[0, direction, step - 1, part],
+            recv_sem=sems.at[1, direction, step - 1, part],
+            device_id=(ahead if direction == 0 else behind, tp),
+            device_id_type=MESH,
+        )
+
+    started = []
+
+    def go(copy):
+        copy.start()
+        started.append(copy)
+
+    def parts_of(step, direction):
+        first = direction
+        return (first,) if step == half else (first, 1 - first)
+
+    for slot in range(2):
+        for direction in range(2):
+            parts = parts_of(1, direction)
+            if slot < len(parts):
+                go(send(direction, 1, parts[slot]))
+    tok_here = pl.ds(pl.multiple_of(tp * count, count), count)
+    for step in range(1, n_tp):
+        go(
+            pltpu.make_async_remote_copy(
+                src_ref=normed_ref,
+                dst_ref=rows_ref.at[tok_here],
+                send_sem=tok_sems.at[0, step - 1],
+                recv_sem=tok_sems.at[1, step - 1],
+                device_id=(sp, lax.rem(tp + step, n_tp)),
+                device_id_type=MESH,
+            )
+        )
+    rows_ref[tok_here, :] = normed_ref[...]
+    for step in range(1, n_tp):
+        origin = pl.ds(pl.multiple_of(lax.rem(tp + n_tp - step, n_tp) * count, count), count)
+        pltpu.make_async_remote_copy(
+            src_ref=normed_ref,
+            dst_ref=rows_ref.at[origin],
+            send_sem=tok_sems.at[0, step - 1],
+            recv_sem=tok_sems.at[1, step - 1],
+            device_id=(sp, lax.rem(tp + step, n_tp)),
+            device_id_type=MESH,
+        ).wait_recv()
+
+    blockwise = depth % LANES == 0
+
+    def add(member, weights, first=False):
+        columns = pl.ds(pl.multiple_of(member * depth, depth), depth)
+        product = jnp.dot(rows_ref[:, columns], weights, preferred_element_type=jnp.float32)
+        total[...] = product if first else total[...] + product
+
+    if blockwise:
+        add(sp, pack_ref[...], True)
+    else:
+        held[rows_of(sp), :] = pack_ref[...]
+    for step in range(1, half + 1):
+        for slot in range(2):
+            for direction in range(2):
+                parts = parts_of(step, direction)
+                if slot < len(parts):
+                    arrival(direction, step, parts[slot]).wait_recv()
+                    if step < half and parts[slot] in parts_of(step + 1, direction):
+                        go(send(direction, step + 1, parts[slot]))
+        if blockwise:
+            for direction in range(1 if step == half else 2):
+                member = owner(direction, step)
+                add(member, held[rows_of(member), :])
+    if not blockwise:
+        total[...] = jnp.dot(rows_ref[...], held[...], preferred_element_type=jnp.float32)
+    out_ref[...] = total[...].astype(out_ref.dtype)
+    for copy in started:
+        copy.wait_send()
+
+
+def project(normed, pack, n, n_tp):
+    depth, width = pack.shape
+    count = normed.shape[0]
+    features = normed.shape[1]
+    vmem = pl.BlockSpec(memory_space=pltpu.VMEM)
+    return pl.pallas_call(
+        functools.partial(project_kernel, n, n_tp),
+        out_shape=jax.ShapeDtypeStruct((n_tp * count, width), jnp.bfloat16),
+        in_specs=[vmem, vmem],
+        out_specs=vmem,
+        scratch_shapes=[
+            pltpu.VMEM((n_tp * count, features), jnp.bfloat16),
+            pltpu.VMEM((n * depth, width), jnp.bfloat16),
+            pltpu.VMEM((n_tp * count, width), jnp.float32),
+            pltpu.SemaphoreType.DMA((2, 2, n // 2, 2)),
+            pltpu.SemaphoreType.DMA((2, n_tp - 1)),
+        ],
+        compiler_params=pltpu.CompilerParams(
+            collective_id=0, has_side_effects=True, vmem_limit_bytes=40 * 2**20
+        ),
+        cost_estimate=pl.CostEstimate(
+            flops=400 * 2**30, bytes_accessed=n * depth * width * 2, transcendentals=0
+        ),
+        name="project_ring",
+    )(normed, pack)
+
+
+def merge_kernel(n_tp, mix_ref, weight_ref, out_ref, outgoing, incoming, sent, landed, sems):
+    sp, tp = lax.axis_index("sp"), lax.axis_index("tp")
+    outer, inner = tp // 2, lax.rem(tp, 2)
+    groups = n_tp // 2
+    count = out_ref.shape[0]
+    barrier = pltpu.get_barrier_semaphore()
+    mate = outer * 2 + 1 - inner
+    pl.semaphore_signal(barrier, inc=1, device_id=(sp, mate), device_id_type=MESH)
+    for step in range(1, groups):
+        peer = lax.rem(outer + step, groups) * 2 + inner
+        pl.semaphore_signal(barrier, inc=1, device_id=(sp, peer), device_id_type=MESH)
+    pl.semaphore_wait(barrier, groups)
+
+    outgoing[...] = jnp.dot(
+        mix_ref[1 - inner], weight_ref[...], preferred_element_type=jnp.float32
+    ).astype(jnp.bfloat16)
+    swap = pltpu.make_async_remote_copy(
+        src_ref=outgoing,
+        dst_ref=incoming,
+        send_sem=sems.at[0, 0],
+        recv_sem=sems.at[1, 0],
+        device_id=(sp, mate),
+        device_id_type=MESH,
+    )
+    swap.start()
+    own = jnp.dot(mix_ref[inner], weight_ref[...], preferred_element_type=jnp.float32)
+    swap.wait_recv()
+    own = own + incoming[...].astype(jnp.float32)
+    sent[...] = own.astype(jnp.bfloat16)
+    copies = []
+    for step in range(1, groups):
+        other = lax.rem(outer + step, groups)
+        copy = pltpu.make_async_remote_copy(
+            src_ref=sent.at[pl.ds(pl.multiple_of(other * count, count), count)],
+            dst_ref=landed.at[step - 1],
+            send_sem=sems.at[0, step],
+            recv_sem=sems.at[1, step],
+            device_id=(sp, other * 2 + inner),
+            device_id_type=MESH,
+        )
+        copy.start()
+        copies.append(copy)
+    mine = sent[pl.ds(pl.multiple_of(outer * count, count), count), :].astype(jnp.float32)
+    for step, copy in enumerate(copies):
+        copy.wait_recv()
+        mine = mine + landed[step].astype(jnp.float32)
+    out_ref[...] = mine.astype(out_ref.dtype)
+    swap.wait_send()
+    for copy in copies:
+        copy.wait_send()
+
+
+def merge(mix, weight, n_tp):
+    rows = mix.shape[0]
+    groups = n_tp // 2
+    count = rows // n_tp
+    width = weight.shape[1]
+    mix = mix.reshape(groups, 2, count, mix.shape[1]).transpose(1, 0, 2, 3)
+    mix = mix.reshape(2, groups * count, -1)
+    vmem = pl.BlockSpec(memory_space=pltpu.VMEM)
+    return pl.pallas_call(
+        functools.partial(merge_kernel, n_tp),
+        out_shape=jax.ShapeDtypeStruct((count, width), jnp.bfloat16),
+        in_specs=[vmem, vmem],
+        out_specs=vmem,
+        scratch_shapes=[
+            pltpu.VMEM((groups * count, width), jnp.bfloat16),
+            pltpu.VMEM((groups * count, width), jnp.bfloat16),
+            pltpu.VMEM((groups * count, width), jnp.bfloat16),
+            pltpu.VMEM((max(1, groups - 1), count, width), jnp.bfloat16),
+            pltpu.SemaphoreType.DMA((2, groups)),
+        ],
+        compiler_params=pltpu.CompilerParams(
+            collective_id=1, has_side_effects=True, vmem_limit_bytes=40 * 2**20
+        ),
+        cost_estimate=pl.CostEstimate(
+            flops=2 * rows * weight.shape[0] * width, bytes_accessed=2 * weight.size, transcendentals=0
+        ),
+        name="merge_scatter",
+    )(mix, weight)
 
 
 def on_device(
@@ -165,21 +411,12 @@
         * lax.rsqrt(jnp.mean(tok_float * tok_float, axis=-1, keepdims=True) + epsilon)
         * norm_gain
     ).astype(jnp.bfloat16)
+    n, n_tp = lax.axis_size("sp"), lax.axis_size("tp")
     weights = (ret_query, ret_key, ret_value, att_query, att_key, att_value)
     widths = [weight.shape[1] for weight in weights]
     points = [sum(widths[:index]) for index in range(1, len(widths))]
-    gathered = (
-        lax.all_gather(weights[0], "sp", axis=0, tiled=True),
-        lax.all_gather(weights[1], "sp", axis=0, tiled=True),
-        lax.all_gather(weights[2], "sp", axis=0, tiled=True),
-        lax.all_gather(weights[3], "sp", axis=0, tiled=True),
-        lax.all_gather(weights[4], "sp", axis=0, tiled=True),
-        lax.all_gather(weights[5], "sp", axis=0, tiled=True),
-    )
-    joined = jnp.concatenate(gathered, axis=1)
-    projected = jnp.dot(
-        lax.all_gather(normed, "tp", axis=0, tiled=True), joined, preferred_element_type=jnp.float32
-    ).astype(jnp.bfloat16)
+    out_whole = lax.all_gather(jnp.concatenate([ret_out, att_out], axis=0), "sp", axis=1, tiled=True)
+    projected = project(normed, jnp.concatenate(weights, axis=1), n, n_tp)
     sections = jnp.split(projected, points, axis=1)
     tok_count = sections[0].shape[0]
     anchor = lax.axis_index("sp") * tok_count
@@ -194,19 +431,7 @@
     value_ret = sections[2].reshape(tok_count, -1, V_DIM)
     ret_mix = retention_path(query_ret, key_ret, value_ret, log_decay)
     att_mix = attention_path(sections[3], sections[4], sections[5], sink_logits, anchor)
-    out_whole = (
-        lax.all_gather(ret_out, "sp", axis=1, tiled=True),
-        lax.all_gather(att_out, "sp", axis=1, tiled=True),
-    )
-    return lax.psum_scatter(
-        (
-            jnp.dot(ret_mix, out_whole[0], preferred_element_type=jnp.float32)
-            + jnp.dot(att_mix, out_whole[1], preferred_element_type=jnp.float32)
-        ).astype(jnp.bfloat16),
-        "tp",
-        scatter_dimension=0,
-        tiled=True,
-    )
+    return merge(jnp.concatenate([ret_mix, att_mix], axis=1), out_whole, n_tp)
 
 
 def solution(mesh):

time: 404 us -> 234 us (0.58)
  waiting for transfers between devices: 266 us -> 94.2 us
  Pallas kernels: 0 us -> 82.8 us
  blocking collectives: 84.1 us -> 18.7 us
  matrix products: 13.5 us -> 2.59 us
  local copies, waits for them, and re-layouts: 15.8 us -> 10.9 us
    all_gather x7 -> x1, waiting for transfers between devices: 219 us -> 73.4 us  [on_device(): lax.all_gather(jnp.concatenate([ret_out, att_out], axis=0), 'sp', axis=1,...]
    pallas_call x0 -> x2, Pallas kernels: none -> 82.8 us  [the longest x1 70.9 us: project(): pl.pallas_call(functools.partial(project_kernel, n, n_tp), out_shape=jax....]
    all_gather x2 -> x0, blocking collectives: 64.4 us -> none  [the longest x1 33.4 us: on_device(): lax.all_gather(weights[4], 'sp', axis=0, tiled=True)]
    reduce_scatter x1 -> x0, waiting for transfers between devices: 23.1 us -> none  [on_device(): lax.psum_scatter((jnp.dot(ret_mix, out_whole[0], preferred_element_type=j...]
    dot_general x3 -> x0, matrix products: 10.9 us -> none  [the longest x1 5.33 us: on_device(): jnp.dot(lax.all_gather(normed, 'tp', axis=0, tiled=True), joined, preferr...]
    concatenate x1, local copies, waits for them, and re-layouts: 11.2 us -> 1.33 us  [on_device(): projected = project(normed, jnp.concatenate(weights, axis=1), n, n_tp)]
    unnamed x15 -> x23, local copies, waits for them, and re-layouts: 1.56 us -> 6.53 us
  transfers between devices with their start and end apart: 10 -> 3, of which waited for: 8 -> 2; matrix products, arithmetic and copies ran while one was open for 6% -> 3% of each run, Pallas kernels for 0% -> 0%
where the time goes in v1:
time: 234 us
  waiting for transfers between devices  94.2 us (40%)
  Pallas kernels  82.8 us (35%)
  blocking collectives  18.7 us (8%)
  between operations  14.5 us (6%)
  local copies, waits for them, and re-layouts  10.9 us (5%)
  other arithmetic  6.4 us (3%)
  starting transfers between devices  3.52 us (2%)
  matrix products  2.59 us (1%)
    all_gather x1, waiting for transfers between devices, on_device(): lax.all_gather(jnp.concatenate([ret_out, att_out], axis=0), 'sp', axis=1,...  73.4 us
    pallas_call x1, Pallas kernels, project(): pl.pallas_call(functools.partial(project_kernel, n, n_tp), out_shape=jax....  70.9 us
    all_gather x1, waiting for transfers between devices, prefix(): gathered = jax.tree.map(lambda a: lax.all_gather(a, axis), part)  20.7 us
    unnamed x1, blocking collectives  18.7 us
    pallas_call x1, Pallas kernels, merge(): pl.pallas_call(functools.partial(merge_kernel, n_tp), out_shape=jax.Shape...  11.9 us
    unnamed x23, local copies, waits for them, and re-layouts  6.53 us
  transfers between devices with their start and end apart: 3, of which 2 were waited for; matrix products, arithmetic and copies ran while one was open for 3% of the time, Pallas kernels for 0%

profile of v1, /device:TPU:0, one launch (start us, length us, event | category | flops | bytes accessed | tf_op | source)
XLA Modules:
  0.0 233.7 jit_solution(1874883892304093340)
XLA Ops:
  6.5 0.5 multiply_power_fusion
  7.1 0.9 copy.55
  7.9 0.9 copy.56
  8.8 1.1 fusion.6
  9.9 1.1 fusion.8.normed_ref
  11.0 1.3 concatenate.36.pack_ref
  12.4 70.9 %project_ring.1 = bf16[256,1664]{1,0:T(8,128)(2,1)S(1)} custom-call(bf16[64,2048]{1,0:T(8,128)(2,1)S(1)} %fusion.8.normed_ref, bf16[256,1664]{1,0:T(8,128)(2,1)S(1)} %concatenate.36.pack_ref), custom_call_target="tpu_custom_call" | custom-call | flops 429496729600 | bytes 6815744 | tf_op jit(solution)/shard_map/project_ring/pallas_call | solution.py:290
  83.6 0.3 copy-done.6
  83.9 0.3 multiply_cosine_fusion
  84.8 0.6 reduce_window_sum.24
  86.2 0.4 fusion.22
  86.6 0.3 while.26
  86.9 0.7 copy-done.1
  87.7 0.8 pad_maximum_fusion
  88.6 3.5 %collective-permute-start = (bf16[128,128]{1,0:T(8,128)(2,1)S(1)}, bf16[128,128]{1,0:T(8,128)(2,1)S(1)}, u32[]{:S(2)}, u32[]{:S(2)}) collective-permute-start(bf16[128,128]{1,0:T(8,128)(2,1)S(1)} %slice.41), channel_id=1, source_target_pairs={{0,4},{4,8},{8,12},{12,16},{16,20},{20,24},{24,28},{1,5},{5,9},{9,... | collective-permute-start | bytes 98312 | tf_op jit(solution)/shard_map/ppermute | solution.py:41
  92.1 0.6 dynamic-slice
  93.7 0.2 fusion.20
  94.0 18.7 %all-reduce = f32[16]{0:T(128)S(1)} all-reduce(f32[16]{0:T(128)S(1)} %exponential_dynamic-update-slice_fusion), channel_id=2, replica_groups=mesh['sp'=8,'tp'=4] {'sp'}, use_global_device_ids=true, to_apply=%add | all-reduce | flops 16 | bytes 128
  113.4 0.3 reshape.265
  113.9 0.5 fusion.52
  114.5 0.3 fusion.1
  114.9 0.5 fusion.3
  115.4 0.2 reshape.266
  115.7 0.4 copy.96
  116.1 20.7 %all-gather.7.cloned.1.call-done = f32[16,128,256]{2,1,0:T(8,128)} async-done(((f32[2,128,256]{2,1,0:T(8,128)}), f32[16,128,256]{2,1,0:T(8,128)}) %all-gather.7.cloned.1.call-update) | async-done | bytes 2097168 | tf_op jit(solution)/shard_map/all_gather | solution.py:27
  136.9 0.8 fusion.10
  137.6 0.5 multiply_reduce_fusion
  138.2 0.2 copy.75
  138.6 73.4 %all-gather.5.cloned.1.call-done.weight_ref = bf16[1024,2048]{1,0:T(8,128)(2,1)} async-done(((bf16[1024,256]{1,0:T(8,128)(2,1)}), bf16[1024,2048]{1,0:T(8,128)(2,1)}) %all-gather.5.cloned.1.call-update) | async-done | bytes 4194320 | tf_op jit(solution)/shard_map/all_gather | solution.py:418
  212.1 2.2 copy-done
  214.3 11.9 %merge_scatter.1 = bf16[64,2048]{1,0:T(8,128)(2,1)S(1)} custom-call(bf16[2,128,1024]{2,1,0:T(8,128)(2,1)S(1)} %bitcast.79, bf16[1024,2048]{1,0:T(8,128)(2,1)S(1)} %copy-done), custom_call_target="tpu_custom_call" | custom-call | flops 1073741824 | bytes 4194304 | tf_op jit(solution)/shard_map/merge_scatter/pallas_call | solution.py:372
  226.2 0.7 copy.127
  (77 shorter events, 3.6 us)
Async XLA Ops:
  6.5 130.3 %all-gather.7.cloned.1.call-start = ((), (), s32[]{:S(2)}) async-start(), calls=%async_computation.1 | async-start | bytes 2359296 | tf_op jit(solution)/shard_map/all_gather | solution.py:27
  83.3 0.7 copy-start.6
  83.3 1.5 copy-start.5
  86.6 1.2 copy-start.2
  86.6 1.2 copy-start.3
  86.6 5.5 %copy-start.7 = (u32[32]{0:T(128)S(1)}, u32[32]{0:T(128)}, u32[]{:S(2)}) copy-start(u32[32]{0:T(128)} %constant.79) | copy-start | bytes 388
  86.9 0.7 copy-start.1
  87.7 124.4 %all-gather.5.cloned.1.call-start = ((), (), s32[]{:S(2)}) async-start(), calls=%async_computation | async-start | bytes 4718592 | tf_op jit(solution)/shard_map/all_gather | solution.py:418
  88.6 25.1 %collective-permute-start = (bf16[128,128]{1,0:T(8,128)(2,1)S(1)}, bf16[128,128]{1,0:T(8,128)(2,1)S(1)}, u32[]{:S(2)}, u32[]{:S(2)}) collective-permute-start(bf16[128,128]{1,0:T(8,128)(2,1)S(1)} %slice.41), channel_id=1, source_target_pairs={{0,4},{4,8},{8,12},{12,16},{16,20},{20,24},{24,28},{1,5},{5,9},{9,... | collective-permute-start | bytes 98312 | tf_op jit(solution)/shard_map/ppermute | solution.py:41
  113.4 1.1 copy-start.4
  212.1 2.2 copy-start
Sparse Core Ops, SparseCore 0:
  87.8 48.9 all-gather.6
  138.9 73.1 all-gather.4

commit v2 on v1

--- a/solution.py
+++ b/solution.py
@@ -20,25 +20,6 @@
 epsilon = 1e-05
 rope_base = 10000.0
 masked_out = -1e30
-
-
-def prefix(part, axis, combine, identity):
-    place = lax.axis_index(axis)
-    gathered = jax.tree.map(lambda a: lax.all_gather(a, axis), part)
-    state = jax.tree.map(lambda a, e: jnp.zeros_like(a) + jnp.asarray(e, a.dtype), part, identity)
-
-    def one(lap, state):
-        return combine(
-            state, jax.tree.map(lambda a: lax.dynamic_index_in_dim(a, lap, 0, False), gathered)
-        )
-
-    return lax.fori_loop(0, place, one, state)
-
-
-def shifted(value, axis, steps):
-    count = lax.axis_size(axis)
-    initial, last = (max(0, -steps), min(count, count - steps))
-    return lax.ppermute(value, axis, [(source, source + steps) for source in range(initial, last)])
 
 
 def rotate(values, positions):
@@ -58,14 +39,7 @@
     )
 
 
-def chain_join(earlier_part, later_part):
-    return (
-        earlier_part[0] * later_part[0],
-        later_part[0][:, None, None] * earlier_part[1] + later_part[1],
-    )
-
-
-def retention_path(query_ret, key_ret, value_ret, log_decay):
+def retention_path(query_ret, key_ret, value_ret, log_decay, rim, logs, weights):
     tok_count, heads_here = (query_ret.shape[0], query_ret.shape[1])
     blocks = tok_count // BLOCK
     q_blocks = query_ret.reshape(blocks, BLOCK, heads_here, RETAIN_KEY_SIZE)
@@ -96,11 +70,19 @@
     final_state, before = lax.scan(
         advance, jnp.zeros((heads_here, RETAIN_KEY_SIZE, V_DIM), jnp.float32), (contrib, block_fade)
     )
-    device_fade = jnp.exp(jnp.sum(closing[:, :, 0], axis=1))
-    identity = (jnp.ones_like(device_fade), jnp.zeros_like(final_state))
-    arrived = prefix((device_fade, final_state), "sp", chain_join, identity)
+    n = lax.axis_size("sp")
+    place = lax.axis_index("sp")
+    before_rim, states, *wholes = exchange(
+        rim, final_state.astype(jnp.bfloat16).reshape(2, -1, V_DIM), weights, n
+    )
+    states = states.reshape(n, heads_here, RETAIN_KEY_SIZE, V_DIM)
+    spots = jnp.arange(n)
+    between = (spots[None, :] > spots[:, None]) & (spots[None, :] < place)
+    spans = jnp.sum(jnp.where(between[:, :, None], logs[None], 0.0), axis=1)
+    shares = jnp.where((spots < place)[:, None], jnp.exp(spans), 0.0)
+    arrived = jnp.sum(shares[:, :, None, None] * states.astype(jnp.float32), axis=0)
     leading = jnp.cumsum(closing[:, :, 0], axis=1) - closing[:, :, 0]
-    before = before + arrived[1][None] * jnp.exp(leading).T[:, :, None, None]
+    before = before + arrived[None] * jnp.exp(leading).T[:, :, None, None]
     query_fade = (
         q_blocks.astype(jnp.float32) * jnp.exp(running).transpose(1, 2, 0)[..., None]
     ).astype(jnp.bfloat16)
@@ -111,15 +93,13 @@
     final_product = final_product * lax.rsqrt(
         jnp.mean(final_product * final_product, axis=-1, keepdims=True) + epsilon
     )
-    return final_product.reshape(tok_count, heads_here * V_DIM).astype(jnp.bfloat16)
-
-
-def attention_path(query_att, key_att, value_att, sink_logits, anchor):
+    return final_product.reshape(tok_count, heads_here * V_DIM).astype(jnp.bfloat16), before_rim, wholes
+
+
+def attention_path(query_att, stacked, window_rim, sink_logits, anchor):
     tok_count = query_att.shape[0]
-    kv_here = key_att.shape[1] // HEAD_DIM
+    kv_here = stacked.shape[1] // (2 * HEAD_DIM)
     group_size = query_att.shape[1] // (kv_here * HEAD_DIM)
-    stacked = jnp.concatenate([key_att, value_att], axis=1)
-    window_rim = shifted(stacked[tok_count - WINDOW :], "sp", 1)
     blocks = tok_count // WINDOW
     extended = jnp.concatenate([window_rim, stacked], axis=0).reshape(
         blocks + 1, WINDOW, 2, kv_here, HEAD_DIM
@@ -162,7 +142,7 @@
     return jnp.where(spot < half, 2 * spot, 2 * (count - 1 - spot) + 1)
 
 
-def project_kernel(n, n_tp, normed_ref, pack_ref, out_ref, rows_ref, held, total, sems, tok_sems):
+def project_kernel(n, n_tp, normed_ref, pack_ref, log_ref, out_ref, logs_ref, rows_ref, held, total, sems, tok_sems):
     sp, tp = lax.axis_index("sp"), lax.axis_index("tp")
     depth, width = pack_ref.shape
     count = normed_ref.shape[0]
@@ -192,6 +172,15 @@
 
     def send(direction, step, part):
         member = owner(direction, step - 1)
+        if part == 2:
+            return pltpu.make_async_remote_copy(
+                src_ref=log_ref if step == 1 else logs_ref.at[member],
+                dst_ref=logs_ref.at[member],
+                send_sem=sems.at[0, direction, step - 1, part],
+                recv_sem=sems.at[1, direction, step - 1, part],
+                device_id=(ahead if direction == 0 else behind, tp),
+                device_id_type=MESH,
+            )
         source = pack_ref.at[:, spans[part]] if step == 1 else held.at[rows_of(member), spans[part]]
         return pltpu.make_async_remote_copy(
             src_ref=source,
@@ -204,6 +193,15 @@
 
     def arrival(direction, step, part):
         member = owner(direction, step)
+        if part == 2:
+            return pltpu.make_async_remote_copy(
+                src_ref=log_ref,
+                dst_ref=logs_ref.at[member],
+                send_sem=sems.at[0, direction, step - 1, part],
+                recv_sem=sems.at[1, direction, step - 1, part],
+                device_id=(ahead if direction == 0 else behind, tp),
+                device_id_type=MESH,
+            )
         return pltpu.make_async_remote_copy(
             src_ref=held.at[rows_of(member), spans[part]],
             dst_ref=held.at[rows_of(member), spans[part]],
@@ -221,9 +219,11 @@
 
     def parts_of(step, direction):
         first = direction
-        return (first,) if step == half else (first, 1 - first)
-
-    for slot in range(2):
+        if step == half:
+            return (2, first) if direction == 0 else (first,)
+        return (2, first, 1 - first)
+
+    for slot in range(3):
         for direction in range(2):
             parts = parts_of(1, direction)
             if slot < len(parts):
@@ -241,6 +241,7 @@
             )
         )
     rows_ref[tok_here, :] = normed_ref[...]
+    logs_ref[sp] = log_ref[...]
     for step in range(1, n_tp):
         origin = pl.ds(pl.multiple_of(lax.rem(tp + n_tp - step, n_tp) * count, count), count)
         pltpu.make_async_remote_copy(
@@ -264,7 +265,7 @@
     else:
         held[rows_of(sp), :] = pack_ref[...]
     for step in range(1, half + 1):
-        for slot in range(2):
+        for slot in range(3):
             for direction in range(2):
                 parts = parts_of(step, direction)
                 if slot < len(parts):
@@ -282,21 +283,24 @@
         copy.wait_send()
 
 
-def project(normed, pack, n, n_tp):
+def project(normed, pack, logs, n, n_tp):
     depth, width = pack.shape
     count = normed.shape[0]
     features = normed.shape[1]
     vmem = pl.BlockSpec(memory_space=pltpu.VMEM)
     return pl.pallas_call(
         functools.partial(project_kernel, n, n_tp),
-        out_shape=jax.ShapeDtypeStruct((n_tp * count, width), jnp.bfloat16),
-        in_specs=[vmem, vmem],
-        out_specs=vmem,
+        out_shape=(
+            jax.ShapeDtypeStruct((n_tp * count, width), jnp.bfloat16),
+            jax.ShapeDtypeStruct((n,) + logs.shape, jnp.float32),
+        ),
+        in_specs=[vmem, vmem, vmem],
+        out_specs=(vmem, vmem),
         scratch_shapes=[
             pltpu.VMEM((n_tp * count, features), jnp.bfloat16),
             pltpu.VMEM((n * depth, width), jnp.bfloat16),
             pltpu.VMEM((n_tp * count, width), jnp.float32),
-            pltpu.SemaphoreType.DMA((2, 2, n // 2, 2)),
+            pltpu.SemaphoreType.DMA((2, 2, n // 2, 3)),
             pltpu.SemaphoreType.DMA((2, n_tp - 1)),
         ],
         compiler_params=pltpu.CompilerParams(
@@ -306,10 +310,114 @@
             flops=400 * 2**30, bytes_accessed=n * depth * width * 2, transcendentals=0
         ),
         name="project_ring",
-    )(normed, pack)
-
-
-def merge_kernel(n_tp, mix_ref, weight_ref, out_ref, outgoing, incoming, sent, landed, sems):
+    )(normed, pack, logs)
+
+
+def exchange_kernel(n, extra, rim_ref, state_ref, *refs):
+    weight_refs = refs[:extra]
+    before_ref, states_ref = refs[extra : extra + 2]
+    whole_refs = refs[extra + 2 : 2 * extra + 2]
+    sems, rim_sems = refs[2 * extra + 2 :]
+    sources = [state_ref.at[0], state_ref.at[1], *weight_refs]
+    sp, tp = lax.axis_index("sp"), lax.axis_index("tp")
+    half = n // 2
+    spot = ring_spot(sp, n)
+    ahead = ring_member(lax.rem(spot + 1, n), n)
+    behind = ring_member(lax.rem(spot + n - 1, n), n)
+    later, earlier = lax.rem(sp + 1, n), lax.rem(sp + n - 1, n)
+    barrier = pltpu.get_barrier_semaphore()
+    for peer in (ahead, behind, later, earlier):
+        pl.semaphore_signal(barrier, inc=1, device_id=(peer, tp), device_id_type=MESH)
+    pl.semaphore_wait(barrier, 4)
+
+    def owner(direction, distance):
+        shift = n - distance if direction == 0 else distance
+        return ring_member(lax.rem(spot + shift, n), n)
+
+    def parts_of(step, direction):
+        order = []
+        for first in range(0, 2 + extra, 2):
+            order.append(first + direction)
+            if step < half:
+                order.append(first + 1 - direction)
+        return order
+
+    def target(member, part):
+        return states_ref.at[member, part] if part < 2 else whole_refs[part - 2].at[member]
+
+    def hop(direction, step, part, member, source):
+        return pltpu.make_async_remote_copy(
+            src_ref=source,
+            dst_ref=target(member, part),
+            send_sem=sems.at[0, direction, step - 1, part],
+            recv_sem=sems.at[1, direction, step - 1, part],
+            device_id=(ahead if direction == 0 else behind, tp),
+            device_id_type=MESH,
+        )
+
+    started = []
+    rim = pltpu.make_async_remote_copy(
+        src_ref=rim_ref,
+        dst_ref=before_ref,
+        send_sem=rim_sems.at[0],
+        recv_sem=rim_sems.at[1],
+        device_id=(later, tp),
+        device_id_type=MESH,
+    )
+    for slot in range(2 + extra):
+        for direction in range(2):
+            parts = parts_of(1, direction)
+            if slot < len(parts):
+                copy = hop(direction, 1, parts[slot], sp, sources[parts[slot]])
+                copy.start()
+                started.append(copy)
+    rim.start()
+    states_ref[sp] = state_ref[...]
+    for whole, piece in zip(whole_refs, weight_refs):
+        whole[sp] = piece[...]
+    for step in range(1, half + 1):
+        for slot in range(2 + extra):
+            for direction in range(2):
+                parts = parts_of(step, direction)
+                if slot < len(parts):
+                    part = parts[slot]
+                    member = owner(direction, step)
+                    hop(direction, step, part, member, sources[part]).wait_recv()
+                    if step < half and part in parts_of(step + 1, direction):
+                        copy = hop(direction, step + 1, part, member, target(member, part))
+                        copy.start()
+                        started.append(copy)
+    rim.wait()
+    for copy in started:
+        copy.wait_send()
+
+
+def exchange(rim, state, weights, n):
+    vmem = pl.BlockSpec(memory_space=pltpu.VMEM)
+    return pl.pallas_call(
+        functools.partial(exchange_kernel, n, len(weights)),
+        out_shape=(
+            jax.ShapeDtypeStruct(rim.shape, rim.dtype),
+            jax.ShapeDtypeStruct((n,) + state.shape, state.dtype),
+            *[jax.ShapeDtypeStruct((n,) + weight.shape, weight.dtype) for weight in weights],
+        ),
+        in_specs=[vmem] * (2 + len(weights)),
+        out_specs=(vmem,) * (2 + len(weights)),
+        scratch_shapes=[
+            pltpu.SemaphoreType.DMA((2, 2, n // 2, 2 + len(weights))),
+            pltpu.SemaphoreType.DMA((2,)),
+        ],
+        compiler_params=pltpu.CompilerParams(
+            collective_id=2, has_side_effects=True, vmem_limit_bytes=40 * 2**20
+        ),
+        cost_estimate=pl.CostEstimate(
+            flops=20 * 2**30, bytes_accessed=n * state.size * 2, transcendentals=0
+        ),
+        name="state_ring",
+    )(rim, state, *weights)
+
+
+def merge_kernel(n_tp, ret_ref, att_ref, ret_out_ref, att_out_ref, out_ref, total, outgoing, incoming, sent, landed, sems):
     sp, tp = lax.axis_index("sp"), lax.axis_index("tp")
     outer, inner = tp // 2, lax.rem(tp, 2)
     groups = n_tp // 2
@@ -322,9 +430,17 @@
         pl.semaphore_signal(barrier, inc=1, device_id=(sp, peer), device_id_type=MESH)
     pl.semaphore_wait(barrier, groups)
 
-    outgoing[...] = jnp.dot(
-        mix_ref[1 - inner], weight_ref[...], preferred_element_type=jnp.float32
-    ).astype(jnp.bfloat16)
+    blocks, _, width = ret_out_ref.shape
+
+    def partial(side, block):
+        return jnp.dot(
+            ret_ref[side], ret_out_ref[block], preferred_element_type=jnp.float32
+        ) + jnp.dot(att_ref[side], att_out_ref[block], preferred_element_type=jnp.float32)
+
+    for block in range(blocks):
+        outgoing[:, block * width : (block + 1) * width] = partial(1 - inner, block).astype(
+            jnp.bfloat16
+        )
     swap = pltpu.make_async_remote_copy(
         src_ref=outgoing,
         dst_ref=incoming,
@@ -334,9 +450,10 @@
         device_id_type=MESH,
     )
     swap.start()
-    own = jnp.dot(mix_ref[inner], weight_ref[...], preferred_element_type=jnp.float32)
+    for block in range(blocks):
+        total[:, block * width : (block + 1) * width] = partial(inner, block)
     swap.wait_recv()
-    own = own + incoming[...].astype(jnp.float32)
+    own = total[...] + incoming[...].astype(jnp.float32)
     sent[...] = own.astype(jnp.bfloat16)
     copies = []
     for step in range(1, groups):
@@ -361,20 +478,23 @@
         copy.wait_send()
 
 
-def merge(mix, weight, n_tp):
-    rows = mix.shape[0]
+def merge(mixes, weights, n_tp):
+    rows = mixes[0].shape[0]
     groups = n_tp // 2
     count = rows // n_tp
-    width = weight.shape[1]
-    mix = mix.reshape(groups, 2, count, mix.shape[1]).transpose(1, 0, 2, 3)
-    mix = mix.reshape(2, groups * count, -1)
+    width = weights[0].shape[0] * weights[0].shape[2]
+    mixes = [
+        mix.reshape(groups, 2, count, -1).transpose(1, 0, 2, 3).reshape(2, groups * count, -1)
+        for mix in mixes
+    ]
     vmem = pl.BlockSpec(memory_space=pltpu.VMEM)
     return pl.pallas_call(
         functools.partial(merge_kernel, n_tp),
         out_shape=jax.ShapeDtypeStruct((count, width), jnp.bfloat16),
-        in_specs=[vmem, vmem],
+        in_specs=[vmem] * 4,
         out_specs=vmem,
         scratch_shapes=[
+            pltpu.VMEM((groups * count, width), jnp.float32),
             pltpu.VMEM((groups * count, width), jnp.bfloat16),
             pltpu.VMEM((groups * count, width), jnp.bfloat16),
             pltpu.VMEM((groups * count, width), jnp.bfloat16),
@@ -385,10 +505,10 @@
             collective_id=1, has_side_effects=True, vmem_limit_bytes=40 * 2**20
         ),
         cost_estimate=pl.CostEstimate(
-            flops=2 * rows * weight.shape[0] * width, bytes_accessed=2 * weight.size, transcendentals=0
+            flops=4 * rows * weights[0].size // 1, bytes_accessed=4 * weights[0].size, transcendentals=0
         ),
         name="merge_scatter",
-    )(mix, weight)
+    )(*mixes, *weights)
 
 
 def on_device(
@@ -415,8 +535,13 @@
     weights = (ret_query, ret_key, ret_value, att_query, att_key, att_value)
     widths = [weight.shape[1] for weight in weights]
     points = [sum(widths[:index]) for index in range(1, len(widths))]
-    out_whole = lax.all_gather(jnp.concatenate([ret_out, att_out], axis=0), "sp", axis=1, tiled=True)
-    projected = project(normed, jnp.concatenate(weights, axis=1), n, n_tp)
+    aligned = ret_out.shape[1] % LANES == 0
+    local_logs = jnp.sum(log_decay, axis=1)
+    log_tile = jnp.broadcast_to(
+        jnp.pad(local_logs, (0, -local_logs.shape[0] % 8))[:, None], (-(-local_logs.shape[0] // 8) * 8, LANES)
+    )
+    projected, logs = project(normed, jnp.concatenate(weights, axis=1), log_tile, n, n_tp)
+    logs = logs[:, : local_logs.shape[0], 0]
     sections = jnp.split(projected, points, axis=1)
     tok_count = sections[0].shape[0]
     anchor = lax.axis_index("sp") * tok_count
@@ -429,9 +554,22 @@
         * RETAIN_KEY_SIZE ** (-0.5)
     ).astype(jnp.bfloat16)
     value_ret = sections[2].reshape(tok_count, -1, V_DIM)
-    ret_mix = retention_path(query_ret, key_ret, value_ret, log_decay)
-    att_mix = attention_path(sections[3], sections[4], sections[5], sink_logits, anchor)
-    return merge(jnp.concatenate([ret_mix, att_mix], axis=1), out_whole, n_tp)
+    stacked = projected[:, points[3] :]
+    ret_mix, rim, wholes = retention_path(
+        query_ret,
+        key_ret,
+        value_ret,
+        log_decay,
+        stacked[tok_count - WINDOW :],
+        logs,
+        (ret_out, att_out) if aligned else (),
+    )
+    if not aligned:
+        wholes = [
+            lax.all_gather(weight, "sp", axis=1, tiled=True)[None] for weight in (ret_out, att_out)
+        ]
+    att_mix = attention_path(sections[3], stacked, rim, sink_logits, anchor)
+    return merge((ret_mix, att_mix), wholes, n_tp)
 
 
 def solution(mesh):

time: 234 us -> 168 us (0.72)
  waiting for transfers between devices: 94.2 us -> 0 us
  Pallas kernels: 82.8 us -> 135 us
  blocking collectives: 18.7 us -> 0 us
  between operations: 14.5 us -> 0.57 us
  local copies, waits for them, and re-layouts: 10.9 us -> 15.6 us
  other arithmetic: 6.4 us -> 10.9 us
  starting transfers between devices: 3.52 us -> 0 us
  matrix products: 2.59 us -> 5.28 us
    all_gather x2 -> x0, waiting for transfers between devices: 94.2 us -> none  [the longest x1 73.4 us: on_device(): lax.all_gather(jnp.concatenate([ret_out, att_out], axis=0), 'sp', axis=1,...]
    pallas_call x1 -> x2, Pallas kernels: 70.9 us -> 125 us  [the longest x1 71.4 us: project(): pl.pallas_call(functools.partial(project_kernel, n, n_tp), out_shape=(jax...]
    unnamed x1 -> x0, blocking collectives: 18.7 us -> none
    ppermute x1 -> x0, starting transfers between devices: 3.48 us -> none  [shifted(): lax.ppermute(value, axis, [(source, source + steps) for source in range(i...]
    unnamed x23 -> x48, local copies, waits for them, and re-layouts: 6.53 us -> 6.11 us
  transfers between devices with their start and end apart: 3 -> 0, of which waited for: 2 -> 0; matrix products, arithmetic and copies ran while one was open for 3% -> 0% of each run, Pallas kernels for 0% -> 0%
where the time goes in v2:
time: 168 us
  Pallas kernels  135 us (80%)
  local copies, waits for them, and re-layouts  15.6 us (9%)
  other arithmetic  10.9 us (6%)
  matrix products  5.28 us (3%)
    pallas_call x1, Pallas kernels, project(): pl.pallas_call(functools.partial(project_kernel, n, n_tp), out_shape=(jax...  71.4 us
    pallas_call x1, Pallas kernels, exchange(): pl.pallas_call(functools.partial(exchange_kernel, n, len(weights)), out_s...  53.7 us
    pallas_call x1, Pallas kernels, merge(): pl.pallas_call(functools.partial(merge_kernel, n_tp), out_shape=jax.Shape...  10.3 us
    unnamed x48, local copies, waits for them, and re-layouts  6.11 us

profile of v2, /device:TPU:0, one launch (start us, length us, event | category | flops | bytes accessed | tf_op | source)
XLA Modules:
  0.0 167.8 jit_solution(1504293390823768473)
XLA Ops:
  0.0 1.1 fusion.6
  1.1 0.8 reduce_sum.55
  2.7 0.7 reshape.294
  3.4 0.6 reduce_window_sum.24
  4.4 0.6 copy.79
  5.0 0.7 copy.76
  5.7 0.6 copy.70
  6.3 0.6 copy.80
  6.9 0.6 copy.73
  7.6 0.6 iota_compare_fusion
  8.2 0.8 fusion.20
  9.0 0.9 copy.60
  9.9 0.9 copy.61
  10.8 1.0 multiply_cosine_fusion
  11.8 1.1 fusion.8.normed_ref
  12.9 1.3 concatenate.26.pack_ref
  14.2 71.4 %project_ring.1 = (bf16[256,1664]{1,0:T(8,128)(2,1)S(1)}, f32[8,8,128]{2,1,0:T(8,128)S(1)}) custom-call(bf16[64,2048]{1,0:T(8,128)(2,1)S(1)} %fusion.8.normed_ref, bf16[256,1664]{1,0:T(8,128)(2,1)S(1)} %concatenate.26.pack_ref, f32[8,128]{1,0:T(8,128)S(1)} %broadcast_in_dim.59.log_ref), custom_call_target="tpu_custom_call" | custom-call | flops 429496729600 | bytes 6815744 | tf_op jit(solution)/shard_map/project_ring/pallas_call | solution.py:291
  86.1 0.7 copy.87
  87.2 0.8 copy.64
  88.0 0.8 copy.65
  90.2 1.7 %while.13 = (s32[]{:T(128)}, f32[2,128,256]{2,1,0:T(8,128)S(1)}, f32[2,2,128,256]{3,2,1,0:T(8,128)}, f32[2,2]{1,0:T(2,128)S(1)}, f32[2,2,128,256]{3,2,1,0:T(8,128)S(1)}, /*index=5*/s32[]{:T(128)}, s32[]{:T(128)}) while((s32[]{:T(128)}, f32[2,128,256]{2,1,0:T(8,128)S(1)}, f32[2,2,128,256]{3,2,1,0:T(8,128)}, f32[2,2]{1,0:T(2,128)S(1)}, ...), condition=%wide.region_4.5_spmd.clone, body=%wide.region_3.4_spmd.clone.sunk | while | flops 262147 | bytes 1310852 | solution.py:70
  90.2 0.7 bitcast_dynamic-update-slice_fusion.2
  91.0 0.7 bitcast_dynamic-update-slice_fusion.2
  92.0 53.7 %state_ring.1 = (bf16[128,128]{1,0:T(8,128)(2,1)S(1)}, bf16[8,2,128,256]{3,2,1,0:T(8,128)(2,1)S(1)}, bf16[8,512,256]{2,1,0:T(8,128)(2,1)S(1)}, bf16[8,512,256]{2,1,0:T(8,128)(2,1)S(1)}) custom-call(bf16[128,128]{1,0:T(8,128)(2,1)S(1)} %slice.47.rim_ref, bf16[2,128,256]{2,1,0:T(8,128)(2,1)S(1)} %convert_element_type.90.state_ref, ...), custom_call_target="tpu_custom_call" | custom-call | flops 21474836480 | bytes 1048576 | tf_op jit(solution)/shard_map/state_ring/pallas_call | solution.py:397
  145.7 1.3 copy-done
  147.4 0.8 fusion.10
  148.1 2.3 %multiply_reduce_fusion.1 = (f32[2,128,2]{1,2,0:T(2,128)S(1)}, f32[2,128,2,256]{1,3,2,0:T(8,128)}) fusion(f32[2,2,256,128]{3,2,1,0:T(8,128)S(1)} %fusion.10, bf16[2,128,2,128]{3,1,2,0:T(8,128)(2,1)} %copy-done.5, f32[2,2,128]{2,0,1:T(2,128)S(1)} %copy-done.13, pred[128,128]{1,0:T(8,128)(4,1)S(1)} %copy-done.12, bf16[2,128,2,64]{3,1,2,0:T(8,128)(2,1)} %copy.65, ...), kind=kOutput, calls=%fused_computation.23 | convolution fusion | flops 51314176 | bytes 1593344 | tf_op jit(solution)/shard_map/hnij,njhv->nihv/dot_general | solution.py:57
  150.4 1.1 multiply_convert_fusion
  152.2 1.4 fusion.53
  155.2 1.6 copy-done.1
  156.8 10.3 %merge_scatter.1 = bf16[64,2048]{1,0:T(8,128)(2,1)S(1)} custom-call(bf16[2,128,512]{2,1,0:T(8,128)(2,1)S(1)} %bitcast.74, bf16[2,128,512]{2,1,0:T(8,128)(2,1)S(1)} %bitcast.73, bf16[8,512,256]{2,1,0:T(8,128)(2,1)S(1)} %get-tuple-element.45.ret_out_ref, bf16[8,512,256]{2,1,0:T(8,128)(2,1)S(1)} %copy-done.1), custom_call_target="tpu_custom_call" | custom-call | flops 1073741824 | bytes 4194304 | tf_op jit(solution)/shard_map/merge_scatter/pallas_call | solution.py:491
  167.1 0.7 copy.129
  (101 shorter events, 6.1 us)
Async XLA Ops:
  0.0 2.7 %copy-start.20 = (pred[8]{0:T(512)(128)(4,1)}, pred[8]{0:T(512)(128)(4,1)S(1)}, u32[]{:S(2)}) copy-start(pred[8]{0:T(512)(128)(4,1)S(1)} %iota_compare_fusion.2) | copy-start | bytes 28
  14.2 71.6 %copy-start.18 = (pred[8,8]{1,0:T(8,128)(4,1)S(1)}, pred[8,8]{1,0:T(8,128)(4,1)}, u32[]{:S(2)}) copy-start(pred[8,8]{1,0:T(8,128)(4,1)} %fusion.42) | copy-start | bytes 196
  14.2 71.6 %copy-start.21 = (pred[8]{0:T(512)(128)(4,1)S(1)}, pred[8]{0:T(512)(128)(4,1)}, u32[]{:S(2)}) copy-start(pred[8]{0:T(512)(128)(4,1)} %copy-done.20) | copy-start | bytes 28
  85.6 1.4 copy-start.10
  85.7 1.4 copy-start.11
  87.2 2.6 %copy-start.15 = (f32[2,128,2]{1,2,0:T(2,128)S(1)}, f32[2,128,2]{1,2,0:T(2,128)}, u32[]{:S(2)}) copy-start(f32[2,128,2]{1,2,0:T(2,128)} %copy.73) | copy-start | bytes 6148
  88.8 1.3 copy-start.4
  88.8 1.3 copy-start.19
  89.4 0.8 copy-start.5
  90.1 1.8 %copy-start.2 = (bf16[512,256]{1,0:T(8,128)(2,1)S(1)}, bf16[512,256]{1,0:T(8,128)(2,1)}, u32[]{:S(2)}) copy-start(bf16[512,256]{1,0:T(8,128)(2,1)} %refs_0_.1) | copy-start | bytes 786436
  90.1 1.8 %copy-start.3 = (bf16[512,256]{1,0:T(8,128)(2,1)S(1)}, bf16[512,256]{1,0:T(8,128)(2,1)}, u32[]{:S(2)}) copy-start(bf16[512,256]{1,0:T(8,128)(2,1)} %refs_1_.1) | copy-start | bytes 786436
  91.9 55.4 %copy-start.6 = (bf16[2,128,2,64]{3,1,2,0:T(8,128)(2,1)S(1)}, bf16[2,128,2,64]{3,1,2,0:T(8,128)(2,1)}, u32[]{:S(2)}) copy-start(bf16[2,128,2,64]{3,1,2,0:T(8,128)(2,1)} %copy.64) | copy-start | bytes 196612
  91.9 55.4 %copy-start.7 = (bf16[2,128,2,64]{3,1,2,0:T(8,128)(2,1)S(1)}, bf16[2,128,2,64]{3,1,2,0:T(8,128)(2,1)}, u32[]{:S(2)}) copy-start(bf16[2,128,2,64]{3,1,2,0:T(8,128)(2,1)} %copy.65) | copy-start | bytes 196612
  91.9 55.4 %copy-start.8 = (f32[2,2,128,256]{3,2,1,0:T(8,128)S(1)}, f32[2,2,128,256]{3,2,1,0:T(8,128)}, u32[]{:S(2)}) copy-start(f32[2,2,128,256]{3,2,1,0:T(8,128)} %get-tuple-element.40) | copy-start | bytes 1572868
  91.9 55.4 %copy-start.14 = (f32[2,128,2]{1,2,0:T(2,128)S(1)}, f32[2,128,2]{1,2,0:T(2,128)}, u32[]{:S(2)}) copy-start(f32[2,128,2]{1,2,0:T(2,128)} %copy.80) | copy-start | bytes 6148
  92.0 55.4 %copy-start.16 = (f32[2,2]{1,0:T(2,128)S(1)}, f32[2,2]{1,0:T(2,128)}, u32[]{:S(2)}) copy-start(f32[2,2]{1,0:T(2,128)} %copy.79) | copy-start | bytes 52
  145.7 1.3 copy-start
  147.0 1.1 copy-start.12
  147.0 1.1 copy-start.13
  151.7 1.9 %copy-start.17 = (f32[8]{0:T(128)S(1)}, f32[8]{0:T(128)}, u32[]{:S(2)}) copy-start(f32[8]{0:T(128)} %param.23) | copy-start | bytes 100
  152.2 1.9 %copy-start.9 = (bf16[2,128,2,1,64]{1,4,0,3,2:T(8,128)(2,1)S(1)}, bf16[2,128,2,1,64]{1,4,0,3,2:T(8,128)(2,1)}, u32[]{:S(2)}) copy-start(bf16[2,128,2,1,64]{1,4,0,3,2:T(8,128)(2,1)} %copy.87) | copy-start | bytes 196612
  155.2 1.6 copy-start.1
